TPU v7x, 512 devices: a whole 4x8x8 slice. The times are simulated.
512 devices in a mesh: sp: 64 (over z, y), tp: 8 (over x, core).
Axes of the slice: x: 4, y: 8, z: 8, core: 2. Of those that a mesh axis runs over, the one named last changes fastest.
Arguments:
- tokens: bfloat16 [16384, 2048], P(('sp', 'tp')), may hold values from -6 to 6
- norm_gain: float32 [2048], replicated, may hold values from 0.1 to 1.9
- w_query: bfloat16 [2048, 1024], P('sp', 'tp'), may hold values from -0.125 to 0.125
- w_forget: bfloat16 [2048, 1024], P('sp', 'tp'), may hold values from -0.125 to 0.125
- w_value: bfloat16 [2048, 1024], P('sp', 'tp'), may hold values from -0.125 to 0.125
- w_outgate: bfloat16 [2048, 1024], P('sp', 'tp'), may hold values from -0.125 to 0.125
- leak: float32 [1024], P('tp'), may hold values from 1.2207031e-05 to 6.1035156e-05
- decay_shift: float32 [16384, 1024], P('sp', 'tp'), may hold values from -1 to 0
- head_gain: float32 [128], replicated, may hold values from 0.1 to 1.9
- w_glu_value: bfloat16 [2048, 2048], P('sp', 'tp'), may hold values from -0.125 to 0.125
- w_glu_gate: bfloat16 [2048, 2048], P('sp', 'tp'), may hold values from -0.125 to 0.125
- conv_kernel: float32 [31, 2048], P(None, 'tp'), may hold values from -20 to 20
- ln_gain: float32 [2048], P('tp'), may hold values from 0.1 to 1.9
- ln_bias: float32 [2048], P('tp'), may hold values from -3 to 3
- w_out_rec: bfloat16 [1024, 2048], P('tp', 'sp'), may hold values from -0.125 to 0.125
- w_out_conv: bfloat16 [2048, 2048], P('tp', 'sp'), may hold values from -0.09375 to 0.09375
Outputs:
- mixed: bfloat16 [16384, 2048], P(('sp', 'tp'))
All inputs are finite; a program needn't handle non-finite values.
Results may differ from a plain program's by a relative error of at most 0.019.
Values may be sent and summed in bfloat16 or wider, within the bound.
No kernel may reach another device: no remote copies, remote signals or barrier semaphores. Data moves between devices by JAX's collectives and lax.ppermute only.
A program may use at most 64 MiB of HBM per device.

v0:
```python
import jax
import jax.numpy as jnp
from jax import lax
from jax.sharding import Mesh
from jax.sharding import PartitionSpec as P

HEAD_K = 128
HEAD_V = 128
KERNEL = 31
BLOCK = 64
SP = ("sp_0", "sp_1")
SP_TP = ("sp_0", "sp_1", "tp")


def turned_gather(arrays, axis, dims):
    turned = [jnp.moveaxis(a, dim, 0) for a, dim in zip(arrays, dims)]
    widths = [t[0].size for t in turned]
    both = jnp.concatenate([t.reshape(-1, w) for t, w in zip(turned, widths)], axis=1)
    filled = lax.all_gather(both, axis, axis=0, tiled=True)
    pieces = jnp.split(filled, [sum(widths[:k]) for k in range(1, len(widths))], axis=1)
    return tuple(
        (
            jnp.moveaxis(b.reshape(-1, *t.shape[1:]), 0, dim)
            for b, t, dim in zip(pieces, turned, dims)
        )
    )


def from_everyone(value, axis):
    copies = jnp.broadcast_to(value, (lax.axis_size(axis), *value.shape))
    return lax.all_to_all(copies, axis, split_axis=0, concat_axis=0, tiled=True)


def laid_out(pieces, dim):
    lengths = list(pieces.shape[1:])
    lengths[dim] *= pieces.shape[0]
    return jnp.moveaxis(pieces, 0, dim).reshape(lengths)


def gather_directly(value, axis, dim):
    pieces = from_everyone(value, axis)
    return laid_out(pieces, dim)


def neutral_like(value, identity):
    return jax.tree.map(
        lambda a, e: jnp.broadcast_to(jnp.asarray(e, a.dtype), a.shape), value, identity
    )


def collected_together(value, axis):
    leaves = jax.tree.leaves(value)
    order = sorted(range(len(leaves)), key=lambda k: -leaves[k].size)
    width = (1, *leaves[order[0]].shape)[-1]
    lines = [
        jnp.pad(leaves[k].reshape(-1), (0, -leaves[k].size % width)).reshape(-1, width)
        for k in order
    ]
    both, at, found = (lax.all_gather(jnp.concatenate(lines), axis), 0, {})
    for k, line in zip(order, lines):
        piece = both[:, at : at + len(line)].reshape(len(both), -1)
        found[k] = piece[:, : leaves[k].size].reshape(-1, *leaves[k].shape)
        at += len(line)
    numbers = iter(range(len(leaves)))
    return jax.tree.map(lambda _: found[next(numbers)], value)


def entering(value, axes, combine, identity):
    before = start = neutral_like(value, identity)
    subtotal = value
    for axis in reversed(axes):
        peers, position = (lax.axis_size(axis), lax.axis_index(axis))
        pieces = collected_together(
            jax.tree.map(
                lambda part, kind: part.astype(kind), subtotal, (jnp.bfloat16, jnp.bfloat16)
            ),
            axis,
        )
        inside, subtotal = (start, start)
        for k in range(peers):
            passed = k < position
            subtotal = combine(
                subtotal, jax.tree.map(lambda part, own: part[k].astype(own.dtype), pieces, value)
            )
            inside = jax.tree.map(lambda new, old: jnp.where(passed, new, old), subtotal, inside)
        before = combine(inside, before)
    return before


def from_behind(value, axis, steps):
    count = lax.axis_size(axis)
    initial, last = (max(0, -steps), min(count, count - steps))
    return lax.ppermute(value, axis, [(source, source + steps) for source in range(initial, last)])


def over_copies(value, axis):
    return from_everyone(value, axis).sum(axis=0)


def in_one(arrays, axis):
    ravelled, at, done = (jnp.concatenate([a.reshape(-1) for a in arrays]), 0, [])
    subtotal = over_copies(ravelled, axis)
    for a in arrays:
        done.append(subtotal[at : at + a.size].reshape(a.shape))
        at += a.size
    return tuple(done)


def split_up(value, dim, peers):
    before, after = (value.shape[:dim], value.shape[dim + 1 :])
    return jnp.moveaxis(value.reshape(*before, peers, -1, *after), dim, 0)


def sent_and_summed(value, axis, dim):
    pieces = split_up(value, dim, lax.axis_size(axis))
    arrived = lax.all_to_all(pieces, axis, split_axis=0, concat_axis=0, tiled=True)
    return arrived.astype(jnp.float32).sum(axis=0)


def normalize(row_block, norm_gain):
    values_in = row_block.astype(jnp.float32)
    row_scale = lax.rsqrt(jnp.mean(values_in * values_in, axis=1, keepdims=True) + 1e-06)
    return (values_in * row_scale * norm_gain).astype(jnp.bfloat16)


def combine_states(earlier, later):
    return (earlier[0] + later[0], jnp.exp(later[0])[..., None] * earlier[1] + later[1])


def local_recurrence(queries, in_gate, payload_matrix_lines, log_decay):
    row_count, head_count, key_width = queries.shape
    value_width = payload_matrix_lines.shape[2]
    block_count = row_count // BLOCK

    def split_blocks(tensor):
        return tensor.reshape(block_count, BLOCK, head_count, tensor.shape[-1])

    q_blocks = split_blocks(queries)
    k_blocks = split_blocks(in_gate)
    v_blocks = split_blocks(payload_matrix_lines)
    cumulative_sum = jnp.cumsum(split_blocks(log_decay), axis=1)
    causal = jnp.tril(jnp.ones((BLOCK, BLOCK), jnp.float32))
    scores = jnp.einsum(
        "nthk,nshk->nhts", q_blocks * jnp.exp(cumulative_sum), k_blocks * jnp.exp(-cumulative_sum)
    )
    within = jnp.einsum("nhts,nshv->nthv", scores * causal, v_blocks)
    block_finish = cumulative_sum[:, -1]
    contrib = jnp.einsum(
        "nshk,nshv->nhkv", k_blocks * jnp.exp(block_finish[:, None] - cumulative_sum), v_blocks
    )

    def advance(carried_in, inputs):
        state_list, before = carried_in
        query_block, column_block, e_block, added_terms = inputs
        carried_state = jnp.einsum("aub,ubd->aud", query_block * jnp.exp(column_block), state_list)
        device_query = query_block * jnp.exp(column_block + before[None])
        state_list = jnp.exp(e_block)[..., None] * state_list + added_terms
        return ((state_list, before + e_block), (carried_state, device_query))

    initial = (
        jnp.zeros((head_count, key_width, value_width), jnp.float32),
        jnp.zeros((head_count, key_width), jnp.float32),
    )
    (state_list, totals), (carried_state, device_query) = lax.scan(
        advance, initial, (q_blocks, cumulative_sum, block_finish, contrib)
    )
    recurrence_step = (within + carried_state).reshape(row_count, head_count, value_width)
    return (
        recurrence_step,
        device_query.reshape(row_count, head_count, key_width),
        state_list,
        totals,
    )


def on_device(
    tokens,
    norm_gain,
    w_query,
    w_forget,
    w_value,
    w_outgate,
    leak,
    decay_shift,
    head_gain,
    w_glu_value,
    w_glu_gate,
    conv_kernel,
    ln_gain,
    ln_bias,
    w_out_rec,
    w_out_conv,
):
    widths = [
        w_query.shape[1],
        w_forget.shape[1],
        w_value.shape[1],
        w_outgate.shape[1],
        w_glu_value.shape[1],
        w_glu_gate.shape[1],
    ]
    gathered = turned_gather(
        (w_query, w_forget, w_value, w_outgate, w_glu_value, w_glu_gate, w_out_rec, w_out_conv),
        SP,
        (0, 0, 0, 0, 0, 0, 1, 1),
    )
    full_in = gathered[:6]
    out_rec = gathered[6]
    out_conv = gathered[7]
    normed = normalize(gather_directly(tokens, "tp", 0), norm_gain)
    joined = jnp.concatenate(
        [
            jnp.dot(normed, weight, preferred_element_type=jnp.float32).astype(jnp.bfloat16)
            for weight in full_in
        ],
        axis=1,
    )
    projections = []
    column = 0
    for width_now in widths:
        projections.append(joined[:, column : column + width_now])
        column = column + width_now
    query_pre, forget_pre, value_pre, gate_pre, glu_value_pre, glu_gate_pre = projections
    row_count = query_pre.shape[0]
    head_count = query_pre.shape[1] // HEAD_K
    queries = jax.nn.silu(query_pre.astype(jnp.float32))
    in_gate = leak * jax.nn.sigmoid(-forget_pre.astype(jnp.float32))
    log_decay = jnp.log1p(-in_gate) + decay_shift
    recurrence_step, device_query, state_list, totals = local_recurrence(
        queries.reshape(row_count, head_count, HEAD_K),
        in_gate.reshape(row_count, head_count, HEAD_K),
        value_pre.astype(jnp.float32).reshape(row_count, head_count, HEAD_V),
        log_decay.reshape(row_count, head_count, HEAD_K),
    )
    _, incoming_state = entering(
        (totals, state_list),
        SP,
        combine_states,
        (jnp.zeros_like(totals), jnp.zeros_like(state_list)),
    )
    recurrence_step = recurrence_step + jnp.einsum("aub,ubd->aud", device_query, incoming_state)
    scaling = lax.rsqrt(jnp.mean(recurrence_step * recurrence_step, axis=2, keepdims=True) + 1e-06)
    gate_act = jax.nn.silu(gate_pre.astype(jnp.float32)).reshape(row_count, head_count, HEAD_V)
    head_out = (
        (recurrence_step * scaling * head_gain * gate_act)
        .reshape(row_count, head_count * HEAD_V)
        .astype(jnp.bfloat16)
    )
    glu = (
        glu_value_pre.astype(jnp.float32) * jax.nn.sigmoid(glu_gate_pre.astype(jnp.float32))
    ).astype(jnp.bfloat16)
    left_rim = from_behind(glu[row_count - (KERNEL - 1) :], SP, 1)
    extended = jnp.concatenate([left_rim, glu], axis=0).astype(jnp.float32)

    def add_tap(tap_index, accum):
        taps = lax.dynamic_slice_in_dim(conv_kernel, tap_index, 1, 0)
        return accum + taps * lax.dynamic_slice_in_dim(extended, tap_index, row_count, 0)

    conv_sum = lax.fori_loop(0, KERNEL, add_tap, jnp.zeros((row_count, glu.shape[1]), jnp.float32))
    channel_count = conv_sum.shape[1] * lax.axis_size("tp")
    sum_rows, square_rows = in_one(
        (
            jnp.sum(conv_sum, axis=1, keepdims=True),
            jnp.sum(conv_sum * conv_sum, axis=1, keepdims=True),
        ),
        "tp",
    )
    row_mean = sum_rows / channel_count
    centered = conv_sum - row_mean
    row_var = square_rows / channel_count - row_mean * row_mean
    conv_out = jax.nn.silu(centered * lax.rsqrt(row_var + 1e-05) * ln_gain + ln_bias).astype(
        jnp.bfloat16
    )
    mixed = sent_and_summed(
        (
            jnp.dot(head_out, out_rec, preferred_element_type=jnp.float32)
            + jnp.dot(conv_out, out_conv, preferred_element_type=jnp.float32)
        ).astype(jnp.bfloat16),
        "tp",
        0,
    )
    return mixed.astype(jnp.bfloat16)


def solution(mesh):
    torus = Mesh(mesh.devices.reshape(8, 8, mesh.shape["tp"]), ("sp_0", "sp_1", "tp"))
    placed = (
        P(SP_TP, None),
        P(),
        P(SP, "tp"),
        P(SP, "tp"),
        P(SP, "tp"),
        P(SP, "tp"),
        P("tp"),
        P(SP, "tp"),
        P(),
        P(SP, "tp"),
        P(SP, "tp"),
        P(None, "tp"),
        P("tp"),
        P("tp"),
        P("tp", SP),
        P("tp", SP),
    )
    return jax.shard_map(
        on_device, mesh=torus, in_specs=placed, out_specs=P(SP_TP, None), check_vma=False
    )
```

profile of v0, /device:TPU:64, one launch (start us, length us, event | category | flops | bytes accessed | tf_op | source)
XLA Modules:
  0.0 237.1 jit_solution(12225472231829536616)
XLA Ops:
  6.5 0.7 constant_dynamic-update-slice_fusion.7
  9.4 0.7 constant_dynamic-update-slice_fusion.3
  12.9 2.0 broadcast_in_dim.19
  14.9 4.3 %all-to-all-start = ((bf16[8,32,2048]{2,1,0:T(8,128)(2,1)}), bf16[8,32,2048]{2,1,0:T(8,128)(2,1)S(1)}, u32[]{:S(2)}, u32[]{:S(2)}) async-start(bf16[8,32,2048]{2,1,0:T(8,128)(2,1)} %broadcast_in_dim.19), calls=%async_computation | async-start | bytes 2097152 | tf_op jit(solution)/shard_map/all_to_all | solution.py:31
  19.3 15.8 %all-to-all-done = bf16[8,32,2048]{2,1,0:T(8,128)(2,1)S(1)} async-done(((bf16[8,32,2048]{2,1,0:T(8,128)(2,1)}), bf16[8,32,2048]{2,1,0:T(8,128)(2,1)S(1)}, u32[]{:S(2)}, u32[]{:S(2)}) %all-to-all-start) | async-done | bytes 1048608 | tf_op jit(solution)/shard_map/all_to_all | solution.py:31
  35.5 1.0 fusion.9
  36.6 69.1 %all-gather.6.cloned.1.call-done = bf16[2048,1408]{1,0:T(8,128)(2,1)} async-done(((bf16[32,1408]{1,0:T(8,128)(2,1)}), bf16[2048,1408]{1,0:T(8,128)(2,1)}) %all-gather.6.cloned.1.call-update) | async-done | bytes 5767184 | tf_op jit(solution)/shard_map/all_gather | solution.py:19
  105.7 1.5 log-plus-one_add_fusion
  107.3 1.5 convolution_convert_fusion.5
  109.0 1.5 divide_multiply_fusion
  110.5 1.5 while.31
  112.1 25.0 %all-gather.2 = bf16[8,129,128]{2,1,0:T(8,128)(2,1)S(1)} all-gather(bf16[1,129,128]{2,1,0:T(8,128)(2,1)S(1)} %maximum_bitcast_fusion), channel_id=2, replica_groups=mesh['sp_0'=8,'sp_1'=8,'tp'=8] {'sp_1'}, dimensions={0}, use_global_device_ids=true | all-gather | bytes 297216 | tf_op jit(solution)/shard_map/all_gather | solution.py:59
  137.3 24.6 %all-gather.3 = bf16[8,129,128]{2,1,0:T(8,128)(2,1)S(1)} all-gather(bf16[1,129,128]{2,1,0:T(8,128)(2,1)S(1)} %maximum_bitcast_fusion.1), channel_id=3, replica_groups=mesh['sp_0'=8,'sp_1'=8,'tp'=8] {'sp_0'}, dimensions={0}, use_global_device_ids=true | all-gather | bytes 297216 | tf_op jit(solution)/shard_map/all_gather | solution.py:59
  162.0 1.7 fusion.17
  163.6 1.7 fusion.16
  165.3 2.7 %collective-permute-start = (bf16[30,256]{1,0:T(8,128)(2,1)S(1)}, bf16[30,256]{1,0:T(8,128)(2,1)S(1)}, u32[]{:S(2)}, u32[]{:S(2)}) collective-permute-start(bf16[30,256]{1,0:T(8,128)(2,1)S(1)} %slice.229), channel_id=1, source_target_pairs={{0,8},{8,16},{16,24},{24,32},{32,40},{40,48},{48,56},{56,64},{64,7... | collective-permute-start | bytes 46088 | tf_op jit(solution)/shard_map/ppermute | solution.py:93
  169.6 3.5 %collective-permute-done = bf16[30,256]{1,0:T(8,128)(2,1)S(1)} collective-permute-done((bf16[30,256]{1,0:T(8,128)(2,1)S(1)}, bf16[30,256]{1,0:T(8,128)(2,1)S(1)}, u32[]{:S(2)}, u32[]{:S(2)}) %collective-permute-start) | collective-permute-done | bytes 15392 | tf_op jit(solution)/shard_map/ppermute | solution.py:93
  173.1 25.7 %while.32 = (s32[]{:T(128)}, f32[256,256]{1,0:T(8,128)S(1)}, f32[31,256]{1,0:T(8,128)}, f32[286,256]{1,0:T(8,128)S(1)}, s32[]{:T(128)}, /*index=5*/s32[]{:T(128)}) while((s32[]{:T(128)}, f32[256,256]{1,0:T(8,128)S(1)}, f32[31,256]{1,0:T(8,128)}, f32[286,256]{1,0:T(8,128)S(1)}, s32[]{:T(128)}, /*index=5*/s32[]{:T(128)}) %tuple.82), condition=%wide.region_6.7_spmd.clone, body=%wide.region_5.6_spmd.clone.sunk | while | flops 196611 | bytes 789591 | solution.py:259
  199.6 4.3 %all-to-all-start.1 = ((f32[8,1,512]{2,1,0:T(1,128)}), f32[8,1,512]{2,1,0:T(1,128)S(1)}, u32[]{:S(2)}, u32[]{:S(2)}) async-start(f32[8,1,512]{2,1,0:T(1,128)} %broadcast_in_dim.23), calls=%async_computation.1 | async-start | bytes 32768 | tf_op jit(solution)/shard_map/all_to_all | solution.py:31
  203.9 2.0 fusion.30
  205.9 3.3 %all-to-all-done.1 = f32[8,1,512]{2,1,0:T(1,128)S(1)} async-done(((f32[8,1,512]{2,1,0:T(1,128)}), f32[8,1,512]{2,1,0:T(1,128)S(1)}, u32[]{:S(2)}, u32[]{:S(2)}) %all-to-all-start.1) | async-done | bytes 16416 | tf_op jit(solution)/shard_map/all_to_all | solution.py:31
  209.3 1.8 fusion.7
  211.1 18.4 %all_to_all.16 = bf16[8,32,2048]{2,1,0:T(8,128)(2,1)S(1)} all-to-all(bf16[8,32,2048]{2,1,0:T(8,128)(2,1)S(1)} %bitcast.158), channel_id=1, replica_groups=mesh['sp_0'=8,'sp_1'=8,'tp'=8] {'tp'}, dimensions={0} | all-to-all | bytes 2097152 | tf_op jit(solution)/shard_map/all_to_all | solution.py:116
  229.4 0.8 reduce_sum.62
  (126 shorter events, 34.8 us)
Async XLA Ops:
  6.5 99.2 %copy-start.2 = (f32[128]{0:T(128)S(1)}, f32[128]{0:T(128)}, u32[]{:S(2)}) copy-start(f32[128]{0:T(128)} %param.26) | copy-start | bytes 1540
  6.5 99.2 %copy-start.1 = (f32[256,128]{1,0:T(8,128)S(1)}, f32[256,128]{1,0:T(8,128)}, u32[]{:S(2)}) copy-start(f32[256,128]{1,0:T(8,128)} %param.27) | copy-start | bytes 393220
  6.5 99.2 %all-gather.6.cloned.1.call-start = ((), (), s32[]{:S(2)}) async-start(), calls=%async_computation.3 | async-start | bytes 5857280 | tf_op jit(solution)/shard_map/all_gather | solution.py:19
  12.3 0.6 copy-start
  14.9 20.2 %all-to-all-start = ((bf16[8,32,2048]{2,1,0:T(8,128)(2,1)}), bf16[8,32,2048]{2,1,0:T(8,128)(2,1)S(1)}, u32[]{:S(2)}, u32[]{:S(2)}) async-start(bf16[8,32,2048]{2,1,0:T(8,128)(2,1)} %broadcast_in_dim.19), calls=%async_computation | async-start | bytes 2097152 | tf_op jit(solution)/shard_map/all_to_all | solution.py:31
  165.3 7.7 %collective-permute-start = (bf16[30,256]{1,0:T(8,128)(2,1)S(1)}, bf16[30,256]{1,0:T(8,128)(2,1)S(1)}, u32[]{:S(2)}, u32[]{:S(2)}) collective-permute-start(bf16[30,256]{1,0:T(8,128)(2,1)S(1)} %slice.229), channel_id=1, source_target_pairs={{0,8},{8,16},{16,24},{24,32},{32,40},{40,48},{48,56},{56,64},{64,7... | collective-permute-start | bytes 46088 | tf_op jit(solution)/shard_map/ppermute | solution.py:93
  199.6 9.6 %all-to-all-start.1 = ((f32[8,1,512]{2,1,0:T(1,128)}), f32[8,1,512]{2,1,0:T(1,128)S(1)}, u32[]{:S(2)}, u32[]{:S(2)}) async-start(f32[8,1,512]{2,1,0:T(1,128)} %broadcast_in_dim.23), calls=%async_computation.1 | async-start | bytes 32768 | tf_op jit(solution)/shard_map/all_to_all | solution.py:31
Sparse Core Ops, SparseCore 0:
  13.0 92.6 all-gather.5
where the time goes:
time: 240 us; the launch traced here: 237 us
  waiting for transfers between devices  91.9 us (38%)
  blocking collectives  68 us (28%)
  local copies, waits for them, and re-layouts  31 us (13%)
  between operations  13.7 us (6%)
  matrix products  13.2 us (6%)
  starting transfers between devices  11.2 us (5%)
  other arithmetic  7.44 us (3%)
    all_gather x1, waiting for transfers between devices, turned_gather(): filled = lax.all_gather(both, axis, axis=0, tiled=True)  69.1 us
    all_gather x2, blocking collectives, collected_together(): both, at, found = (lax.all_gather(jnp.concatenate(lines), axis), 0, {})  49.6 us
    dynamic_slice x31, local copies, waits for them, and re-layouts, add_tap(): taps = lax.dynamic_slice_in_dim(conv_kernel, tap_index, 1, 0)  21.9 us
    all_to_all x2, waiting for transfers between devices, from_everyone(): return lax.all_to_all(copies, axis, split_axis=0, concat_axis=0, tiled=True)  19.2 us
    all_to_all x1, blocking collectives, sent_and_summed(): lax.all_to_all(pieces, axis, split_axis=0, concat_axis=0, tiled=True)  18.4 us
    all_to_all x2, starting transfers between devices, from_everyone(): return lax.all_to_all(copies, axis, split_axis=0, concat_axis=0, tiled=True)  8.55 us
    dot_general x5, matrix products, on_device(): jnp.dot(normed, weight, preferred_element_type=jnp.float32)  7.78 us
    unnamed x14, local copies, waits for them, and re-layouts  5.64 us
  transfers between devices with their start and end apart: 4, of which 4 were waited for; matrix products, arithmetic and copies ran while one was open for 3% of the time, Pallas kernels for 0%

commit v1 on v0

--- a/solution.py
+++ b/solution.py
@@ -16,7 +16,9 @@
     turned = [jnp.moveaxis(a, dim, 0) for a, dim in zip(arrays, dims)]
     widths = [t[0].size for t in turned]
     both = jnp.concatenate([t.reshape(-1, w) for t, w in zip(turned, widths)], axis=1)
-    filled = lax.all_gather(both, axis, axis=0, tiled=True)
+    filled = jnp.concatenate(
+        lax.all_to_all(jnp.stack([both] * lax.axis_size(axis)), axis, 0, 0), axis=0
+    )
     pieces = jnp.split(filled, [sum(widths[:k]) for k in range(1, len(widths))], axis=1)
     return tuple(
         (

time: 240 us -> 363 us (1.51)
  waiting for transfers between devices: 91.9 us -> 180 us
  blocking collectives: 68 us -> 101 us
  starting transfers between devices: 11.2 us -> 25.6 us
  between operations: 13.7 us -> 0.32 us
    all_to_all x0 -> x1, waiting for transfers between devices: none -> 162 us  [turned_gather(): lax.all_to_all(jnp.stack([both] * lax.axis_size(axis)), axis, 0, 0)]
    all_gather x1 -> x0, waiting for transfers between devices: 69.1 us -> none  [turned_gather(): filled = lax.all_gather(both, axis, axis=0, tiled=True)]
    all_gather x2, blocking collectives: 49.6 us -> 82.6 us  [collected_together(): both, at, found = (lax.all_gather(jnp.concatenate(lines), axis), 0, {})]
    all_to_all x0 -> x1, starting transfers between devices: none -> 16.1 us  [turned_gather(): lax.all_to_all(jnp.stack([both] * lax.axis_size(axis)), axis, 0, 0)]
    all_to_all x2, waiting for transfers between devices: 19.2 us -> 13.5 us  [from_everyone(): return lax.all_to_all(copies, axis, split_axis=0, concat_axis=0, tiled=True)]
where the time goes in v1:
time: 363 us; the launch traced here: 360 us
  waiting for transfers between devices  180 us (50%)
  blocking collectives  101 us (28%)
  local copies, waits for them, and re-layouts  33.3 us (9%)
  starting transfers between devices  25.6 us (7%)
  matrix products  13.2 us (4%)
  other arithmetic  6.73 us (2%)
    all_to_all x1, waiting for transfers between devices, turned_gather(): lax.all_to_all(jnp.stack([both] * lax.axis_size(axis)), axis, 0, 0)  162 us
    all_gather x2, blocking collectives, collected_together(): both, at, found = (lax.all_gather(jnp.concatenate(lines), axis), 0, {})  82.6 us
    dynamic_slice x31, local copies, waits for them, and re-layouts, add_tap(): taps = lax.dynamic_slice_in_dim(conv_kernel, tap_index, 1, 0)  21.9 us
    all_to_all x1, blocking collectives, sent_and_summed(): lax.all_to_all(pieces, axis, split_axis=0, concat_axis=0, tiled=True)  18.4 us
    all_to_all x1, starting transfers between devices, turned_gather(): lax.all_to_all(jnp.stack([both] * lax.axis_size(axis)), axis, 0, 0)  16.1 us
    all_to_all x2, waiting for transfers between devices, from_everyone(): return lax.all_to_all(copies, axis, split_axis=0, concat_axis=0, tiled=True)  13.5 us
    dot_general x5, matrix products, on_device(): jnp.dot(normed, weight, preferred_element_type=jnp.float32)  7.78 us
    all_to_all x2, starting transfers between devices, from_everyone(): return lax.all_to_all(copies, axis, split_axis=0, concat_axis=0, tiled=True)  7.64 us
  transfers between devices with their start and end apart: 4, of which 4 were waited for; matrix products, arithmetic and copies ran while one was open for 3% of the time, Pallas kernels for 0%

profile of v1, /device:TPU:64, one launch (start us, length us, event | category | flops | bytes accessed | tf_op | source)
XLA Modules:
  0.0 360.4 jit_solution(10920414817887679624)
XLA Ops:
  0.0 2.0 broadcast_in_dim.19
  2.0 4.3 %all-to-all-start = ((bf16[8,32,2048]{2,1,0:T(8,128)(2,1)}), bf16[8,32,2048]{2,1,0:T(8,128)(2,1)S(1)}, u32[]{:S(2)}, u32[]{:S(2)}) async-start(bf16[8,32,2048]{2,1,0:T(8,128)(2,1)} %broadcast_in_dim.19), calls=%async_computation | async-start | bytes 2097152 | tf_op jit(solution)/shard_map/all_to_all | solution.py:33
  9.1 0.7 constant_dynamic-update-slice_fusion.3
  12.0 10.3 %all-to-all-done = bf16[8,32,2048]{2,1,0:T(8,128)(2,1)S(1)} async-done(((bf16[8,32,2048]{2,1,0:T(8,128)(2,1)}), bf16[8,32,2048]{2,1,0:T(8,128)(2,1)S(1)}, u32[]{:S(2)}, u32[]{:S(2)}) %all-to-all-start) | async-done | bytes 1048608 | tf_op jit(solution)/shard_map/all_to_all | solution.py:33
  22.2 3.0 stack.2
  25.2 16.1 %all-to-all-start.1 = ((bf16[64,32,1408]{2,1,0:T(8,128)(2,1)}), bf16[64,32,1408]{2,1,0:T(8,128)(2,1)}, u32[]{:S(2)}, u32[]{:S(2)}) async-start(bf16[64,32,1408]{2,1,0:T(8,128)(2,1)} %stack.2), calls=%async_computation.1 | async-start | bytes 11534336 | tf_op jit(solution)/shard_map/all_to_all | solution.py:20
  42.1 161.7 %all-to-all-done.1 = bf16[64,32,1408]{2,1,0:T(8,128)(2,1)} async-done(((bf16[64,32,1408]{2,1,0:T(8,128)(2,1)}), bf16[64,32,1408]{2,1,0:T(8,128)(2,1)}, u32[]{:S(2)}, u32[]{:S(2)}) %all-to-all-start.1) | async-done | bytes 5767200 | tf_op jit(solution)/shard_map/all_to_all | solution.py:20
  203.8 1.5 convolution_convert_fusion.5
  205.3 1.5 divide_multiply_fusion
  206.8 1.7 fusion.17
  208.5 1.5 log-plus-one_add_fusion
  210.3 1.5 while.31
  211.9 45.3 %all-gather.2 = bf16[8,129,128]{2,1,0:T(8,128)(2,1)S(1)} all-gather(bf16[1,129,128]{2,1,0:T(8,128)(2,1)S(1)} %maximum_bitcast_fusion), channel_id=2, replica_groups=mesh['sp_0'=8,'sp_1'=8,'tp'=8] {'sp_1'}, dimensions={0}, use_global_device_ids=true | all-gather | bytes 297216 | tf_op jit(solution)/shard_map/all_gather | solution.py:61
  257.5 37.3 %all-gather.3 = bf16[8,129,128]{2,1,0:T(8,128)(2,1)S(1)} all-gather(bf16[1,129,128]{2,1,0:T(8,128)(2,1)S(1)} %maximum_bitcast_fusion.1), channel_id=3, replica_groups=mesh['sp_0'=8,'sp_1'=8,'tp'=8] {'sp_0'}, dimensions={0}, use_global_device_ids=true | all-gather | bytes 297216 | tf_op jit(solution)/shard_map/all_gather | solution.py:61
  294.7 1.7 fusion.16
  296.5 1.9 collective-permute-start
  299.9 4.3 %collective-permute-done = bf16[30,256]{1,0:T(8,128)(2,1)S(1)} collective-permute-done((bf16[30,256]{1,0:T(8,128)(2,1)S(1)}, bf16[30,256]{1,0:T(8,128)(2,1)S(1)}, u32[]{:S(2)}, u32[]{:S(2)}) %collective-permute-start) | collective-permute-done | bytes 15392 | tf_op jit(solution)/shard_map/ppermute | solution.py:95
  304.2 25.7 %while.32 = (s32[]{:T(128)}, f32[256,256]{1,0:T(8,128)S(1)}, f32[31,256]{1,0:T(8,128)}, f32[286,256]{1,0:T(8,128)S(1)}, s32[]{:T(128)}, /*index=5*/s32[]{:T(128)}) while((s32[]{:T(128)}, f32[256,256]{1,0:T(8,128)S(1)}, f32[31,256]{1,0:T(8,128)}, f32[286,256]{1,0:T(8,128)S(1)}, s32[]{:T(128)}, /*index=5*/s32[]{:T(128)}) %tuple.82), condition=%wide.region_6.7_spmd.clone, body=%wide.region_5.6_spmd.clone.sunk | while | flops 196611 | bytes 789599 | solution.py:261
  330.7 3.3 all-to-all-start.2
  334.1 2.0 fusion.30
  336.1 3.3 all-to-all-done.2
  339.4 1.8 fusion.7
  341.2 18.4 %all_to_all.21 = bf16[8,32,2048]{2,1,0:T(8,128)(2,1)S(1)} all-to-all(bf16[8,32,2048]{2,1,0:T(8,128)(2,1)S(1)} %bitcast.159), channel_id=1, replica_groups=mesh['sp_0'=8,'sp_1'=8,'tp'=8] {'tp'}, dimensions={0} | all-to-all | bytes 2097152 | tf_op jit(solution)/shard_map/all_to_all | solution.py:118
  359.6 0.8 reduce_sum.62
  (126 shorter events, 35.2 us)
Async XLA Ops:
  2.0 20.2 %all-to-all-start = ((bf16[8,32,2048]{2,1,0:T(8,128)(2,1)}), bf16[8,32,2048]{2,1,0:T(8,128)(2,1)S(1)}, u32[]{:S(2)}, u32[]{:S(2)}) async-start(bf16[8,32,2048]{2,1,0:T(8,128)(2,1)} %broadcast_in_dim.19), calls=%async_computation | async-start | bytes 2097152 | tf_op jit(solution)/shard_map/all_to_all | solution.py:33
  25.2 16.6 %copy-start = (f32[2048]{0:T(1024)S(1)}, f32[2048]{0:T(1024)}, u32[]{:S(2)}) copy-start(f32[2048]{0:T(1024)} %param.21) | copy-start | bytes 24580
  25.2 178.6 %all-to-all-start.1 = ((bf16[64,32,1408]{2,1,0:T(8,128)(2,1)}), bf16[64,32,1408]{2,1,0:T(8,128)(2,1)}, u32[]{:S(2)}, u32[]{:S(2)}) async-start(bf16[64,32,1408]{2,1,0:T(8,128)(2,1)} %stack.2), calls=%async_computation.1 | async-start | bytes 11534336 | tf_op jit(solution)/shard_map/all_to_all | solution.py:20
  41.3 167.1 %copy-start.1 = (f32[256,128]{1,0:T(8,128)S(1)}, f32[256,128]{1,0:T(8,128)}, u32[]{:S(2)}) copy-start(f32[256,128]{1,0:T(8,128)} %param.27) | copy-start | bytes 393220
  41.3 167.1 %copy-start.2 = (f32[128]{0:T(128)S(1)}, f32[128]{0:T(128)}, u32[]{:S(2)}) copy-start(f32[128]{0:T(128)} %param.26) | copy-start | bytes 1540
  296.5 7.7 %collective-permute-start = (bf16[30,256]{1,0:T(8,128)(2,1)S(1)}, bf16[30,256]{1,0:T(8,128)(2,1)S(1)}, u32[]{:S(2)}, u32[]{:S(2)}) collective-permute-start(bf16[30,256]{1,0:T(8,128)(2,1)S(1)} %slice.229), channel_id=1, source_target_pairs={{0,8},{8,16},{16,24},{24,32},{32,40},{40,48},{48,56},{56,64},{64,7... | collective-permute-start | bytes 46088 | tf_op jit(solution)/shard_map/ppermute | solution.py:95
  330.7 8.6 %all-to-all-start.2 = ((f32[8,1,512]{2,1,0:T(1,128)}), f32[8,1,512]{2,1,0:T(1,128)S(1)}, u32[]{:S(2)}, u32[]{:S(2)}) async-start(f32[8,1,512]{2,1,0:T(1,128)} %broadcast_in_dim.23), calls=%async_computation.2 | async-start | bytes 32768 | tf_op jit(solution)/shard_map/all_to_all | solution.py:33
